TPU v7x, 128 devices: a whole 4x4x4 slice. The times are simulated.
128 devices in a mesh: ep: 32 (over z, y, core), tp: 4 (over x).
Axes of the slice: x: 4, y: 4, z: 4, core: 2. Of those that a mesh axis runs over, the one named last changes fastest.
Arguments:
- hidden: bfloat16 [2048, 2048], P('ep'), may hold values from -10 to 10
- mix_gain: bfloat16 [2048], replicated, may hold values from 0.099609375 to 1.8984375
- proj_x: bfloat16 [2048, 2048], P('ep', 'tp'), may hold values from -0.125 to 0.125
- proj_y: bfloat16 [2048, 2048], P('ep', 'tp'), may hold values from -0.125 to 0.125
- conv_taps: bfloat16 [4, 2048], P(None, 'tp'), may hold values from -3 to 3
- input_gate: bfloat16 [32, 64, 64], P('tp'), may hold values from -0.75 to 0.75
- decay_gate: bfloat16 [32, 64, 64], P('tp'), may hold values from -0.75 to 0.75
- decay_param: float32 [2048], P('tp'), may hold values from 1 to 6
- proj_out: bfloat16 [2048, 2048], P('tp'), may hold values from -0.125 to 0.125
- conv_state: bfloat16 [2048, 3, 2048], P('ep', None, 'tp'), may hold values from -6 to 6
- lru_state: float32 [2048, 2048], P('ep', 'tp'), may hold values from -6 to 6
- ffn_gain: bfloat16 [2048], replicated, may hold values from 0.099609375 to 1.8984375
- routes: int32 [2048, 2], P('ep'), may hold values from 0 to 31, all different within a row; in each aligned block of 64 rows (0 to 63, 64 to 127, ...) at most 6 rows name the same one
- route_weights: float32 [2048, 2], P('ep'), may hold values from 0.2 to 1
- expert_gate: bfloat16 [32, 2048, 3072], P('ep', None, 'tp'), may hold values from -0.125 to 0.125
- expert_up: bfloat16 [32, 2048, 3072], P('ep', None, 'tp'), may hold values from -0.125 to 0.125
- expert_down: bfloat16 [32, 3072, 2048], P('ep', 'tp'), may hold values from -0.109375 to 0.109375
- dense_gate: bfloat16 [2048, 6144], P('tp', 'ep'), may hold values from -0.125 to 0.125
- dense_up: bfloat16 [2048, 6144], P('tp', 'ep'), may hold values from -0.125 to 0.125
- dense_down: bfloat16 [6144, 2048], P('ep', 'tp'), may hold values from -0.078125 to 0.078125
- branch_gate: float32 [2048], P('tp'), may hold values from -4 to 4
Outputs:
- new_hidden: bfloat16 [2048, 2048], P('ep', 'tp')
- new_lru: float32 [2048, 2048], P('ep', 'tp')
- new_conv: bfloat16 [2048, 3, 2048], P('ep', None, 'tp')
Inputs may be any that keep to these rules, and one draw needn't show every extreme that they name: `routes`: each row names 2 different experts. In the 64 rows of one index of ep, no expert is named by more than 6 rows, a bound that some block reaches.
All inputs are finite; a program needn't handle non-finite values.
Results may differ from a plain program's by a relative error of at most 0.017.
Values may be sent and summed in bfloat16 or wider, within the bound.
A program may use at most 128 MiB of HBM per device.

v0:
```python
import jax
import jax.numpy as jnp
from jax import lax
from jax.sharding import PartitionSpec as P

epsilon = 1e-06
decay_scale = 8.0


def in_one_piece(arrays, axis, dim, along):
    widths = [a.shape[along] for a in arrays]
    both = jnp.concatenate(arrays, axis=along)
    whole = lax.all_gather(both, axis, axis=dim, tiled=True)
    return tuple(jnp.split(whole, [sum(widths[:k]) for k in range(1, len(widths))], axis=along))


def split_up(value, dim, devices):
    before, after = (value.shape[:dim], value.shape[dim + 1 :])
    return jnp.moveaxis(value.reshape(*before, devices, -1, *after), dim, 0)


def sum_at_owner(value, axis, dim):
    devices = lax.axis_size(axis)
    blocks = lax.all_to_all(split_up(value, dim, devices), axis, 0, 0, tiled=True)
    return jnp.sum(blocks.astype(jnp.float32), axis=0)


def in_order(blocks, dim):
    blocks = jnp.moveaxis(blocks, 0, dim)
    shape = blocks.shape
    return blocks.reshape(*shape[:dim], shape[dim] * shape[dim + 1], *shape[dim + 2 :])


def copy_for_each(value, axis):
    copies = jnp.broadcast_to(value, (lax.axis_size(axis), *value.shape))
    return lax.all_to_all(copies, axis, split_axis=0, concat_axis=0, tiled=True)


def gathered_copies(value, axis, dim):
    return in_order(copy_for_each(value, axis), dim)


def rms_scale(values, gain_vec):
    floats = values.astype(jnp.float32)
    meansq = jnp.mean(floats * floats, axis=-1, keepdims=True)
    return floats * lax.rsqrt(meansq + epsilon) * gain_vec.astype(jnp.float32)


def on_device(
    hidden,
    mix_gain,
    proj_x,
    proj_y,
    conv_taps,
    input_gate,
    decay_gate,
    decay_param,
    proj_out,
    conv_state,
    lru_state,
    ffn_gain,
    routes,
    route_weights,
    expert_gate,
    expert_up,
    expert_down,
    dense_gate,
    dense_up,
    dense_down,
    branch_gate,
):
    tok_rows = hidden.shape[0]
    ep_size = lax.axis_size("ep")
    tp_size = lax.axis_size("tp")
    col_width = hidden.shape[1] // tp_size
    col_start = lax.axis_index("tp") * col_width
    lru_local = lru_state.shape[1]
    normed = rms_scale(hidden, mix_gain).astype(jnp.bfloat16)
    pieces = in_one_piece((proj_x, proj_y), "ep", 0, 1)
    x_total = jnp.dot(normed, pieces[0], preferred_element_type=jnp.float32)
    y_total = jnp.dot(normed, pieces[1], preferred_element_type=jnp.float32)
    x_proj = x_total.astype(jnp.bfloat16)
    y_proj = y_total.astype(jnp.bfloat16)
    window = jnp.concatenate([conv_state, x_proj[:, None, :]], axis=1)
    conv_out = jnp.sum(
        window.astype(jnp.float32) * conv_taps.astype(jnp.float32)[None], axis=1
    ).astype(jnp.bfloat16)
    heads_here = input_gate.shape[0]
    block_size = input_gate.shape[1]
    heads_in = conv_out.reshape(tok_rows, heads_here, block_size)
    gate_in = jax.nn.sigmoid(
        jnp.einsum(
            "bhi,hij->bhj", heads_in, input_gate, preferred_element_type=jnp.float32
        ).reshape(tok_rows, lru_local)
    )
    gate_dec = jax.nn.sigmoid(
        jnp.einsum(
            "bhi,hij->bhj", heads_in, decay_gate, preferred_element_type=jnp.float32
        ).reshape(tok_rows, lru_local)
    )
    log_decay = decay_scale * gate_dec * jax.nn.log_sigmoid(decay_param)
    decay_rate = jnp.exp(log_decay)
    inject = jnp.sqrt(-jnp.expm1(2.0 * log_decay))
    new_lru = decay_rate * lru_state + inject * gate_in * conv_out.astype(jnp.float32)
    gated_out = (new_lru * jax.nn.gelu(y_proj.astype(jnp.float32))).astype(jnp.bfloat16)
    partial_value = jnp.dot(gated_out, proj_out, preferred_element_type=jnp.float32)
    mixer_sum = sum_at_owner(partial_value.astype(jnp.bfloat16), "tp", 1)
    own_hidden = lax.dynamic_slice_in_dim(hidden, col_start, col_width, 1)
    summed = (own_hidden.astype(jnp.float32) + mixer_sum).astype(jnp.bfloat16)
    whole_rows = gathered_copies(summed, "tp", 1)
    ffn_in = rms_scale(whole_rows, ffn_gain).astype(jnp.bfloat16)
    ffn_cols = lax.dynamic_slice_in_dim(ffn_in, col_start, col_width, 1)
    top_count = routes.shape[1]
    local_experts = expert_gate.shape[0]
    experts_all = local_experts * ep_size
    capacity = tok_rows * top_count // experts_all + 2
    pair_expert = routes.reshape(-1)
    onehot = (pair_expert[:, None] == jnp.arange(experts_all, dtype=jnp.int32)[None, :]).astype(
        jnp.int32
    )
    slot_rank = jnp.sum((jnp.cumsum(onehot, axis=0) - onehot) * onehot, axis=1)
    slot_index = pair_expert * capacity + slot_rank
    select = (
        slot_index[:, None] == jnp.arange(experts_all * capacity, dtype=jnp.int32)[None, :]
    ).astype(jnp.bfloat16)
    pair_rows = jnp.repeat(ffn_in, top_count, axis=0)
    dispatch = jnp.einsum(
        "pe,pd->ed", select, pair_rows, preferred_element_type=jnp.float32
    ).astype(jnp.bfloat16)
    dispatch = dispatch.reshape(experts_all, capacity, ffn_in.shape[1])
    arrived = lax.all_to_all(dispatch, "ep", split_axis=0, concat_axis=0, tiled=True)
    items = arrived.shape[1]
    grouped = arrived.reshape(ep_size, local_experts, items, arrived.shape[2])
    gate_val = jnp.einsum(
        "sgid,gdf->sgif", grouped, expert_gate, preferred_element_type=jnp.float32
    )
    up_val = jnp.einsum("sgid,gdf->sgif", grouped, expert_up, preferred_element_type=jnp.float32)
    inner_act = (jax.nn.silu(gate_val) * up_val).astype(jnp.bfloat16)
    partial_out = jnp.einsum(
        "sgif,gfd->sgid", inner_act, expert_down, preferred_element_type=jnp.float32
    )
    reduced = sum_at_owner(partial_out.astype(jnp.bfloat16), "tp", 3).astype(jnp.bfloat16)
    flat_back = reduced.reshape(ep_size * local_experts, items, reduced.shape[3])
    returned = lax.all_to_all(flat_back, "ep", split_axis=0, concat_axis=0, tiled=True)
    weighted = select.astype(jnp.float32) * route_weights.reshape(-1)[:, None]
    per_token = jnp.sum(weighted.reshape(tok_rows, top_count, experts_all * capacity), axis=1)
    expert_sum = jnp.dot(
        per_token,
        returned.reshape(experts_all * capacity, col_width).astype(jnp.float32),
        precision=lax.Precision.HIGHEST,
    )
    dense_both = jnp.concatenate([dense_gate, dense_up], axis=1)
    ff_local = dense_gate.shape[1]
    dense_part = jnp.dot(
        gathered_copies(ffn_cols, "ep", 0), dense_both, preferred_element_type=jnp.float32
    )
    dense_full = lax.psum(dense_part.astype(jnp.bfloat16), "tp").astype(jnp.float32)
    dense_act = (jax.nn.silu(dense_full[:, :ff_local]) * dense_full[:, ff_local:]).astype(
        jnp.bfloat16
    )
    dense_out = lax.psum_scatter(
        jnp.dot(dense_act, dense_down, preferred_element_type=jnp.float32).astype(jnp.bfloat16),
        "ep",
        scatter_dimension=0,
        tiled=True,
    ).astype(jnp.float32)
    new_hidden = (
        summed.astype(jnp.float32) + expert_sum + jax.nn.sigmoid(branch_gate)[None, :] * dense_out
    ).astype(jnp.bfloat16)
    return (new_hidden, new_lru, window[:, 1:])


def solution(mesh):
    in_specs = (
        P("ep", None),
        P(),
        P("ep", "tp"),
        P("ep", "tp"),
        P(None, "tp"),
        P("tp", None, None),
        P("tp", None, None),
        P("tp"),
        P("tp", None),
        P("ep", None, "tp"),
        P("ep", "tp"),
        P(),
        P("ep", None),
        P("ep", None),
        P("ep", None, "tp"),
        P("ep", None, "tp"),
        P("ep", "tp", None),
        P("tp", "ep"),
        P("tp", "ep"),
        P("ep", "tp"),
        P("tp"),
    )
    out_specs = (P("ep", "tp"), P("ep", "tp"), P("ep", None, "tp"))
    return jax.shard_map(
        on_device, mesh=mesh, in_specs=in_specs, out_specs=out_specs, check_vma=False
    )
```

profile of v0, /device:TPU:1, one launch (start us, length us, event | category | flops | bytes accessed | tf_op | source)
XLA Modules:
  0.0 277.6 jit_solution(10338469871885520587)
XLA Ops:
  12.2 48.5 %all-gather.2.cloned.1.call-done = bf16[2048,1024]{1,0:T(8,128)(2,1)} async-done(((bf16[64,1024]{1,0:T(8,128)(2,1)}), bf16[2048,1024]{1,0:T(8,128)(2,1)}) %all-gather.2.cloned.1.call-update) | async-done | bytes 4194320 | tf_op jit(solution)/shard_map/all_gather | solution.py:13
  60.7 2.2 fusion.48
  71.6 1.8 multiply_add_fusion
  73.4 4.0 %convolution_convert_fusion.3 = bf16[64,2048]{1,0:T(8,128)(2,1)} fusion(bf16[512,2048]{1,0:T(8,128)(2,1)} %param.29, f32[64,512]{1,0:T(8,128)} %multiply_add_fusion, bf16[2048,1024]{1,0:T(8,128)(2,1)} %all-gather.2.cloned.1.call-done, bf16[64,2048]{1,0:T(8,128)(2,1)S(1)} %copy-done.1, f32[2048]{0:T(1024)S(1)} %convert_element_type.123, ...), kind=kOutput, calls=%fused_computation.10 | convolution fusion | flops 269484032 | bytes 4858112 | tf_op jit(solution)/shard_map/dot_general | solution.py:106
  79.1 4.0 %all-to-all-start = ((bf16[4,64,512]{2,1,0:T(8,128)(2,1)}), bf16[4,64,512]{2,1,0:T(8,128)(2,1)}, u32[]{:S(2)}, u32[]{:S(2)}) async-start(bf16[4,64,512]{2,1,0:T(8,128)(2,1)} %bitcast.92), calls=%async_computation | async-start | bytes 524288 | tf_op jit(solution)/shard_map/all_to_all | solution.py:24
  83.1 6.0 %all-to-all-done = bf16[4,64,512]{2,1,0:T(8,128)(2,1)} async-done(((bf16[4,64,512]{2,1,0:T(8,128)(2,1)}), bf16[4,64,512]{2,1,0:T(8,128)(2,1)}, u32[]{:S(2)}, u32[]{:S(2)}) %all-to-all-start) | async-done | bytes 262176 | tf_op jit(solution)/shard_map/all_to_all | solution.py:24
  90.9 3.4 %all-to-all-start.1 = ((bf16[4,64,512]{2,1,0:T(8,128)(2,1)}), bf16[4,64,512]{2,1,0:T(8,128)(2,1)S(1)}, u32[]{:S(2)}, u32[]{:S(2)}) async-start(bf16[4,64,512]{2,1,0:T(8,128)(2,1)} %broadcast_in_dim.9), calls=%async_computation.1 | async-start | bytes 524288 | tf_op jit(solution)/shard_map/all_to_all | solution.py:36
  94.3 5.4 %all-to-all-done.1 = bf16[4,64,512]{2,1,0:T(8,128)(2,1)S(1)} async-done(((bf16[4,64,512]{2,1,0:T(8,128)(2,1)}), bf16[4,64,512]{2,1,0:T(8,128)(2,1)S(1)}, u32[]{:S(2)}, u32[]{:S(2)}) %all-to-all-start.1) | async-done | bytes 262176 | tf_op jit(solution)/shard_map/all_to_all | solution.py:36
  100.4 36.1 %all_to_all.30 = bf16[32,64,512]{2,1,0:T(8,128)(2,1)S(1)} all-to-all(bf16[32,64,512]{2,1,0:T(8,128)(2,1)S(1)} %broadcast_in_dim.11), channel_id=1, replica_groups=mesh['ep'=32,'tp'=4] {'ep'}, dimensions={0} | all-to-all | bytes 4194304 | tf_op jit(solution)/shard_map/all_to_all | solution.py:36
  136.5 2.4 convolution_convert_fusion.1
  139.3 45.7 %all-reduce.2.cloned.1.call-done = bf16[2048,384]{1,0:T(8,128)(2,1)} async-done(((bf16[2048,384]{1,0:T(8,128)(2,1)}), bf16[2048,384]{1,0:T(8,128)(2,1)}) %all-reduce.2.cloned.1.call-update) | async-done | bytes 1572880 | tf_op jit(solution)/shard_map/psum | solution.py:157
  186.7 2.3 convolution_convert_fusion
  192.0 2.0 reshape.116
  194.1 2.4 convolution_convert_fusion.2
  196.5 2.2 reshape.117
  198.7 24.9 %all_to_all.31 = bf16[32,6,2048]{2,1,0:T(8,128)(2,1)S(1)} all-to-all(bf16[32,6,2048]{2,1,0:T(8,128)(2,1)} %reshape.117), channel_id=1, replica_groups=mesh['ep'=32,'tp'=4] {'ep'}, dimensions={0} | all-to-all | bytes 1572864 | tf_op jit(solution)/shard_map/all_to_all | solution.py:131
  224.5 4.0 %fusion.14 = f32[32,1,6,768]{3,0,2,1:T(8,128)} fusion(bf16[1,2048,768]{2,1,0:T(8,128)(2,1)} %param.35, bf16[32,6,2048]{2,1,0:T(8,128)(2,1)S(1)} %all_to_all.31), kind=kOutput, calls=%fused_computation.17 | convolution fusion | flops 603979776 | bytes 4521984 | tf_op jit(solution)/shard_map/sgid,gdf->sgif/dot_general | solution.py:134
  228.5 5.1 %fusion.6 = bf16[32,6,2048]{2,0,1:T(8,128)(2,1)} fusion(bf16[1,768,2048]{2,1,0:T(8,128)(2,1)S(1)} %copy-done, bf16[1,2048,768]{2,1,0:T(8,128)(2,1)} %param.36, f32[32,1,6,768]{3,0,2,1:T(8,128)} %fusion.14, bf16[32,6,2048]{2,1,0:T(8,128)(2,1)} %copy-done.2), kind=kOutput, calls=%fused_computation.8 | convolution fusion | flops 1209237504 | bytes 8454144 | tf_op jit(solution)/shard_map/sgif,gfd->sgid/dot_general | solution.py:139
  233.7 2.3 copy.113
  235.9 4.3 %all-to-all-start.3 = ((bf16[4,32,1,6,512]{4,1,3,2,0:T(8,128)(2,1)}), bf16[4,32,1,6,512]{4,1,3,2,0:T(8,128)(2,1)}, u32[]{:S(2)}, u32[]{:S(2)}) async-start(bf16[4,32,1,6,512]{4,1,3,2,0:T(8,128)(2,1)} %bitcast.88), calls=%async_computation.3 | async-start | bytes 1572864 | tf_op jit(solution)/shard_map/all_to_all | solution.py:24
  240.5 11.8 %all-to-all-done.3 = bf16[4,32,1,6,512]{4,1,3,2,0:T(8,128)(2,1)} async-done(((bf16[4,32,1,6,512]{4,1,3,2,0:T(8,128)(2,1)}), bf16[4,32,1,6,512]{4,1,3,2,0:T(8,128)(2,1)}, u32[]{:S(2)}, u32[]{:S(2)}) %all-to-all-start.3) | async-done | bytes 786464 | tf_op jit(solution)/shard_map/all_to_all | solution.py:24
  254.5 4.8 %all-to-all-start.4 = ((bf16[32,6,512]{2,1,0:T(8,128)(2,1)}), bf16[32,6,512]{2,1,0:T(8,128)(2,1)S(1)}, u32[]{:S(2)}, u32[]{:S(2)}) async-start(bf16[32,6,512]{2,1,0:T(8,128)(2,1)} %copy.97), calls=%async_computation.4 | async-start | bytes 524288 | tf_op jit(solution)/shard_map/all_to_all | solution.py:144
  261.0 7.5 %all-to-all-done.4 = bf16[32,6,512]{2,1,0:T(8,128)(2,1)S(1)} async-done(((bf16[32,6,512]{2,1,0:T(8,128)(2,1)}), bf16[32,6,512]{2,1,0:T(8,128)(2,1)S(1)}, u32[]{:S(2)}, u32[]{:S(2)}) %all-to-all-start.4) | async-done | bytes 196640 | tf_op jit(solution)/shard_map/all_to_all | solution.py:144
  269.3 1.8 fusion.38
  (76 shorter events, 28.6 us)
Async XLA Ops:
  7.2 221.3 %copy-start = (bf16[1,768,2048]{2,1,0:T(8,128)(2,1)S(1)}, bf16[1,768,2048]{2,1,0:T(8,128)(2,1)}, u32[]{:S(2)}) copy-start(bf16[1,768,2048]{2,1,0:T(8,128)(2,1)} %param.37) | copy-start | bytes 9437188
  7.2 55.7 %copy-start.3 = (bf16[64,3,512]{2,0,1:T(8,128)(2,1)S(1)}, bf16[64,3,512]{2,0,1:T(8,128)(2,1)}, u32[]{:S(2)}) copy-start(bf16[64,3,512]{2,0,1:T(8,128)(2,1)} %param.30) | copy-start | bytes 589828
  7.2 53.5 %all-gather.2.cloned.1.call-start = ((), (), s32[]{:S(2)}) async-start(), calls=%async_computation.7 | async-start | bytes 4325376 | tf_op jit(solution)/shard_map/all_gather | solution.py:13
  62.9 0.6 copy-start.4
  63.5 0.7 copy-start.5
  65.3 8.1 %copy-start.1 = (bf16[64,2048]{1,0:T(8,128)(2,1)S(1)}, bf16[64,2048]{1,0:T(8,128)(2,1)}, u32[]{:S(2)}) copy-start(bf16[64,2048]{1,0:T(8,128)(2,1)} %param.21) | copy-start | bytes 786436
  77.4 16.9 %copy-start.6 = (bf16[2048]{0:T(1024)(128)(2,1)S(1)}, bf16[2048]{0:T(1024)(128)(2,1)}, u32[]{:S(2)}) copy-start(bf16[2048]{0:T(1024)(128)(2,1)} %param.32) | copy-start | bytes 12292
  79.1 10.0 %all-to-all-start = ((bf16[4,64,512]{2,1,0:T(8,128)(2,1)}), bf16[4,64,512]{2,1,0:T(8,128)(2,1)}, u32[]{:S(2)}, u32[]{:S(2)}) async-start(bf16[4,64,512]{2,1,0:T(8,128)(2,1)} %bitcast.92), calls=%async_computation | async-start | bytes 524288 | tf_op jit(solution)/shard_map/all_to_all | solution.py:24
  90.9 8.9 %all-to-all-start.1 = ((bf16[4,64,512]{2,1,0:T(8,128)(2,1)}), bf16[4,64,512]{2,1,0:T(8,128)(2,1)S(1)}, u32[]{:S(2)}, u32[]{:S(2)}) async-start(bf16[4,64,512]{2,1,0:T(8,128)(2,1)} %broadcast_in_dim.9), calls=%async_computation.1 | async-start | bytes 524288 | tf_op jit(solution)/shard_map/all_to_all | solution.py:36
  94.3 90.8 %all-reduce.2.cloned.1.call-start = ((), (), s32[]{:S(2)}) async-start(), calls=%async_computation.8 | async-start | bytes 3145728 | tf_op jit(solution)/shard_map/psum | solution.py:157
  100.4 36.1 %copy-start.10 = (bf16[512,192]{0,1:T(8,128)(2,1)S(1)}, bf16[512,192]{0,1:T(8,128)(2,1)}, u32[]{:S(2)}) copy-start(bf16[512,192]{0,1:T(8,128)(2,1)} %param.39) | copy-start | bytes 589828
  100.4 36.1 %copy-start.11 = (bf16[512,192]{0,1:T(8,128)(2,1)S(1)}, bf16[512,192]{0,1:T(8,128)(2,1)}, u32[]{:S(2)}) copy-start(bf16[512,192]{0,1:T(8,128)(2,1)} %param.38) | copy-start | bytes 589828
  136.5 2.5 copy-start.7
  139.0 130.3 %reduce-scatter.2.cloned.1.call-start = ((), (), s32[]{:S(2)}) async-start(), calls=%async_computation.9 | async-start | bytes 2162688 | tf_op jit(solution)/shard_map/reduce_scatter | solution.py:161
  185.0 1.7 copy-start.12
  223.5 1.0 copy-start.2
  233.7 6.8 %copy-start.8 = (f32[512]{0:T(512)S(1)}, f32[512]{0:T(512)}, u32[]{:S(2)}) copy-start(f32[512]{0:T(512)} %param.41) | copy-start | bytes 6148
  235.9 23.4 %copy-start.9 = (f32[64,2]{0,1:T(2,128)S(1)}, f32[64,2]{0,1:T(2,128)}, u32[]{:S(2)}) copy-start(f32[64,2]{0,1:T(2,128)} %param.34) | copy-start | bytes 1540
  235.9 16.4 %all-to-all-start.3 = ((bf16[4,32,1,6,512]{4,1,3,2,0:T(8,128)(2,1)}), bf16[4,32,1,6,512]{4,1,3,2,0:T(8,128)(2,1)}, u32[]{:S(2)}, u32[]{:S(2)}) async-start(bf16[4,32,1,6,512]{4,1,3,2,0:T(8,128)(2,1)} %bitcast.88), calls=%async_computation.3 | async-start | bytes 1572864 | tf_op jit(solution)/shard_map/all_to_all | solution.py:24
  254.5 14.1 %all-to-all-start.4 = ((bf16[32,6,512]{2,1,0:T(8,128)(2,1)}), bf16[32,6,512]{2,1,0:T(8,128)(2,1)S(1)}, u32[]{:S(2)}, u32[]{:S(2)}) async-start(bf16[32,6,512]{2,1,0:T(8,128)(2,1)} %copy.97), calls=%async_computation.4 | async-start | bytes 524288 | tf_op jit(solution)/shard_map/all_to_all | solution.py:144
Sparse Core Ops, SparseCore 0:
  10.8 49.7 all-gather.1
  139.1 45.8 all-reduce.1
  189.1 77.7 reduce-scatter.1
where the time goes:
time: 279 us; the launch traced here: 278 us
  waiting for transfers between devices  125 us (45%)
  blocking collectives  60.9 us (22%)
  matrix products  26.5 us (9%)
  local copies, waits for them, and re-layouts  19.7 us (7%)
  starting transfers between devices  16.7 us (6%)
  other arithmetic  14.7 us (5%)
  between operations  14 us (5%)
    all_gather x1, waiting for transfers between devices, in_one_piece(): whole = lax.all_gather(both, axis, axis=dim, tiled=True)  48.5 us
    psum x1, waiting for transfers between devices, on_device(): lax.psum(dense_part.astype(jnp.bfloat16), 'tp').astype(jnp.float32)  45.7 us
    all_to_all x1, blocking collectives, copy_for_each(): return lax.all_to_all(copies, axis, split_axis=0, concat_axis=0, tiled=True)  36.1 us
    all_to_all x1, blocking collectives, on_device(): lax.all_to_all(dispatch, 'ep', split_axis=0, concat_axis=0, tiled=True)  24.9 us
    all_to_all x2, waiting for transfers between devices, sum_at_owner(): lax.all_to_all(split_up(value, dim, devices), axis, 0, 0, tiled=True)  17.8 us
    all_to_all x2, starting transfers between devices, sum_at_owner(): lax.all_to_all(split_up(value, dim, devices), axis, 0, 0, tiled=True)  8.36 us
    all_to_all x1, waiting for transfers between devices, on_device(): lax.all_to_all(flat_back, 'ep', split_axis=0, concat_axis=0, tiled=True)  7.48 us
  transfers between devices with their start and end apart: 7, of which 6 were waited for; matrix products, arithmetic and copies ran while one was open for 11% of the time, Pallas kernels for 0%

commit v1 on v0

v1 whole, which is shorter than its diff:
```python
import jax
import jax.numpy as jnp
from jax import lax
from jax.experimental import pallas as pl
from jax.experimental.pallas import tpu as pltpu
from jax.sharding import PartitionSpec as P

MESH = pl.DeviceIdType.MESH
F32 = jnp.float32
BF16 = jnp.bfloat16
I32 = jnp.int32

epsilon = 1e-06
decay_scale = 8.0
D = 2048
COLS = 512
OFFS = (0, -1, 1, 2)


def dot(a, b):
    return jnp.dot(a, b, preferred_element_type=F32)


def dot_nt(a, b):
    return lax.dot_general(a, b, (((1,), (1,)), ((), ())), preferred_element_type=F32)


def iota(shape, dim):
    return lax.broadcasted_iota(I32, shape, dim)


def mask(cond):
    return jnp.where(cond, 1.0, 0.0)


def div6(v):
    return (v * 171) >> 10


def rms_scale(floats, gain):
    meansq = jnp.mean(floats * floats, axis=-1, keepdims=True)
    return floats * lax.rsqrt(meansq + epsilon) * gain.astype(F32)


def sigmoid(v):
    return 1.0 / (1.0 + jnp.exp(-v))


def neg_expm1(v):
    series = -v * (1.0 + v * (1 / 2) * (1.0 + v * (1 / 3) * (1.0 + v * (1 / 4) * (1.0 + v * (1 / 5)))))
    return jnp.where(v > -0.1, series, 1.0 - jnp.exp(v))


def kernel(
    mix_gain, conv_taps, input_gate, decay_gate, decay_param, ffn_gain, routes, route_weights,
    branch_gate, hidden_h, proj_x_h, proj_y_h, proj_out_h, conv_h, lru_h, eg_h, eu_h, ed_h,
    dg_h, du_h, dd_h,
    new_hidden, new_lru, x_out,
    hid, px, py, wo, conv, lru, eg, eu, ed, dg, du, dd,
    gx, gy, wown, wgu, wd, nrm, bd_in, bd_dec, csum, gout, pp, rsb, smb, sxb, xall, dtok,
    fstack, sel, comb, perm, qmat, disp, arr, xrows, inner, pe, er, ret, back,
    dhid, dpart, drecv, dsb, dxb,
    lsem, ag_s, ag_r, dw_s, dw_r, rs_s, rs_r, xa_s, xa_r, sm_s, sm_r, da_s, da_r,
    di_s, di_r, er_s, er_r, re_s, re_r, dr_s, dr_r, dx_s, dx_r,
):
    ep = lax.axis_index("ep")
    x = lax.axis_index("tp")
    c = lax.rem(ep, 2)
    chip = lax.div(ep, 2)
    y = lax.rem(chip, 4)
    z = lax.div(chip, 4)

    def m4(v):
        return lax.rem(v + 8, 4)

    def cp(src, dst, ssem, rsem, dev):
        return pltpu.make_async_remote_copy(
            src_ref=src, dst_ref=dst, send_sem=ssem, recv_sem=rsem, device_id=dev, device_id_type=MESH
        )

    loads = [
        (proj_x_h, px), (proj_y_h, py), (hidden_h, hid), (dg_h, dg), (du_h, du), (dd_h, dd),
        (conv_h, conv), (lru_h, lru), (proj_out_h, wo), (eg_h.at[0], eg), (eu_h.at[0], eu),
        (ed_h.at[0], ed),
    ]

    def load(k):
        return pltpu.make_async_copy(loads[k][0], loads[k][1], lsem.at[k])

    for k in range(len(loads)):
        load(k).start()

    bar = pltpu.get_barrier_semaphore()

    def greet(k, carry):
        pl.semaphore_signal(bar, inc=1, device_id=(lax.rem(ep + k, 32), x), device_id_type=MESH)
        return carry

    lax.fori_loop(1, 32, greet, 0)
    for k in (1, 2, 3):
        pl.semaphore_signal(bar, inc=1, device_id=(ep, m4(x + k)), device_id_type=MESH)
    load(0).wait()
    load(1).wait()
    pl.semaphore_wait(bar, 34)

    own = (px, py)
    bufs = (gx, gy)
    first = (y, z)
    second = (z, y)

    def chip_of(h, f, s):
        return (s * 4 + f) if h == 0 else (f * 4 + s)

    def slot(h, f, s, cc):
        return bufs[h].at[s, f, cc] if h == 0 else bufs[h].at[f, s, cc]

    def piece(h, f, s, half):
        return slot(h, f, s, c).at[pl.ds(32 * half, 32), :]

    def dev(h, f, s, cc):
        return (chip_of(h, f, s) * 2 + cc, x)

    sent = []

    def go(copy):
        copy.start()
        sent.append(copy)

    def to_f(h, step, idx, src, dst):
        go(cp(src, dst, ag_s.at[h, idx], ag_r.at[h, idx], dev(h, m4(first[h] + step), second[h], c)))

    def to_s(h, step, idx, src, dst):
        go(cp(src, dst, ag_s.at[h, idx], ag_r.at[h, idx], dev(h, first[h], m4(second[h] + step), c)))

    def to_p(h, idx, src, dst):
        go(cp(src, dst, ag_s.at[h, idx], ag_r.at[h, idx], (chip * 2 + 1 - c, x)))

    def got(h, idx, dst):
        cp(dst, dst, ag_s.at[h, idx], ag_r.at[h, idx], (chip * 2 + 1 - c, x)).wait_recv()

    def second_phase(h, i, src):
        f, s = m4(first[h] + OFFS[i]), second[h]
        to_s(h, 1, 4 + 4 * i, src, slot(h, f, s, c))
        to_s(h, -1, 5 + 4 * i, src, slot(h, f, s, c))

    def across(h, i, si, src=None):
        f, s = m4(first[h] + OFFS[i]), m4(second[h] + OFFS[si])
        mine = slot(h, f, s, c)
        to_p(h, 20 + 4 * si + i, mine if src is None else src, mine)

    for h in range(2):
        f, s = first[h], second[h]
        to_f(h, 1, 0, own[h], slot(h, f, s, c))
        to_f(h, -1, 1, own[h], slot(h, f, s, c))
    for h in range(2):
        second_phase(h, 0, own[h])
        across(h, 0, 0, own[h])
    gx[z, y, c] = px[...]
    gy[z, y, c] = py[...]

    r64 = iota((64, 128), 0)
    c128 = iota((64, 128), 1)
    put = (mask(c128 == r64).astype(BF16), mask(c128 == r64 + 64).astype(BF16))

    load(3).wait()
    load(4).wait()
    load(5).wait()
    wown[:, 0:128] = dg[:, 0:128]
    wown[:, 128:256] = du[:, 0:128]
    wown[:, 256:384] = (dot(dg[:, 128:192], put[0]) + dot(du[:, 128:192], put[1])).astype(BF16)

    load(2).wait()
    nrm[...] = rms_scale(hid[...].astype(F32), mix_gain[...]).astype(BF16)

    wsrc = (wown, dd)
    wdst = (wgu, wd)
    wrows = (256, 96)

    def w_go(a, idx, src, dst, device):
        go(cp(src, dst, dw_s.at[a, idx], dw_r.at[a, idx], device))

    def w_got(a, idx, dst):
        cp(dst, dst, dw_s.at[a, idx], dw_r.at[a, idx], (chip * 2 + 1 - c, x)).wait_recv()

    for a in range(2):
        w_go(a, 0, wsrc[a], wdst[a].at[c, x], (ep, m4(x + 1)))
        w_go(a, 1, wsrc[a], wdst[a].at[c, x], (ep, m4(x - 1)))
        w_go(a, 4, wsrc[a], wdst[a].at[c, x], (chip * 2 + 1 - c, x))
    wgu[c, x] = wown[...]
    wd[c, x] = dd[...]

    for h in range(2):
        f, s = first[h], second[h]
        lo, hi = m4(f - 1), m4(f + 1)
        got(h, 0, slot(h, lo, s, c))
        to_f(h, 1, 2, piece(h, lo, s, 0), piece(h, lo, s, 0))
        second_phase(h, 1, slot(h, lo, s, c))
        across(h, 1, 0)
        got(h, 1, slot(h, hi, s, c))
        to_f(h, -1, 3, piece(h, hi, s, 1), piece(h, hi, s, 1))
        second_phase(h, 2, slot(h, hi, s, c))
        across(h, 2, 0)

    def arrivals(h, i):
        f, s = m4(first[h] + OFFS[i]), second[h]
        lo, hi = m4(s - 1), m4(s + 1)
        got(h, 4 + 4 * i, slot(h, f, lo, c))
        to_s(h, 1, 6 + 4 * i, piece(h, f, lo, 0), piece(h, f, lo, 0))
        across(h, i, 1)
        got(h, 5 + 4 * i, slot(h, f, hi, c))
        to_s(h, -1, 7 + 4 * i, piece(h, f, hi, 1), piece(h, f, hi, 1))
        across(h, i, 2)

    def last(h, i):
        f, s = m4(first[h] + OFFS[i]), m4(second[h] + 2)
        got(h, 6 + 4 * i, piece(h, f, s, 0))
        got(h, 7 + 4 * i, piece(h, f, s, 1))
        across(h, i, 3)

    e32 = iota((64, 32), 1)
    oh = [mask(routes[:, r:r + 1] == e32) for r in range(2)]
    both = oh[0] + oh[1]
    lower = mask(iota((64, 64), 1) < iota((64, 64), 0)).astype(BF16)
    rank1 = both * (dot(lower, both.astype(BF16)) + 1.0)
    rank1b = rank1.astype(BF16)

    for h in range(2):
        arrivals(h, 0)
    for h in range(2):
        f, s = m4(first[h] + 2), second[h]
        got(h, 2, piece(h, f, s, 0))
        got(h, 3, piece(h, f, s, 1))
        second_phase(h, 3, slot(h, f, s, c))
        across(h, 3, 0)

    for p in range(4):
        for gate, block in ((input_gate, bd_in), (decay_gate, bd_dec)):
            for k in range(2):
                block[p, 64 * k:64 * k + 64, :] = dot(gate[2 * p + k], put[k]).astype(BF16)

    for h in range(2):
        arrivals(h, 1)

    load(6).wait()
    taps = conv_taps[...].astype(F32)
    csum[...] = jnp.sum(conv[...].astype(F32) * taps[None, 0:3, :], axis=1)

    for h in range(2):
        arrivals(h, 2)

    tt = mask((iota((512, 64), 0) & 63) == iota((512, 64), 1)).astype(BF16)
    spread = dot(tt, rank1b).astype(BF16)
    rows = iota((1536, 32), 0)
    ecol = iota((1536, 32), 1) * 48
    erow = mask((rows >= ecol) & (rows < ecol + 48)).astype(BF16)
    row1 = iota((1536, 1), 0)
    six1 = div6(row1 >> 3)
    rin = row1 - six1 * 48
    ck1 = div6(rin)
    slot1 = (rin - 6 * ck1 + 1).astype(F32)
    ckcol = iota((1536, 512), 1) >> 6
    sel[...] = mask((dot_nt(erow, spread) == slot1) & (ck1 == ckcol)).astype(BF16)

    for h in range(2):
        last(h, 0)
    for h in range(2):
        arrivals(h, 3)

    pr = iota((384, 384), 0)
    pc = iota((384, 384), 1)
    prc = div6(pr >> 3)
    prr = pr - 48 * prc
    prs = div6(prr)
    perm[...] = mask(pc == prs * 48 + prc * 6 + (prr - 6 * prs)).astype(BF16)
    qr = iota((512, 384), 0)
    qc = iota((512, 384), 1)
    qslot = qr & 7
    qmat[...] = mask((qslot < 6) & (qc == ((qr >> 3) & 1) * 192 + (qr >> 4) * 6 + qslot)).astype(BF16)

    for h in range(2):
        last(h, 1)

    w0 = route_weights[:, 0:1]
    w1 = route_weights[:, 1:2]
    wfull = w0 * oh[0] + w1 * oh[1]
    whi = wfull.astype(BF16)
    wlo = (wfull - whi.astype(F32)).astype(BF16)
    expand = mask((iota((32, 512), 1) >> 4) == iota((32, 512), 0)).astype(BF16)
    ccol = iota((64, 512), 1)
    hit = dot(rank1b, expand) == ((ccol & 7) + 1).astype(F32)
    ehi = dot(whi, expand)
    elo = dot(wlo, expand)
    for j in range(2):
        here = hit & (((ccol >> 3) & 1) == j)
        comb[j, 0] = jnp.where(here, ehi, 0.0).astype(BF16)
        comb[j, 1] = jnp.where(here, elo, 0.0).astype(BF16)

    for h in range(2):
        last(h, 2)
    for h in range(2):
        last(h, 3)

    for h in range(2):
        for si in range(4):
            for i in range(4):
                f, s = m4(first[h] + OFFS[i]), m4(second[h] + OFFS[si])
                got(h, 20 + 4 * si + i, slot(h, f, s, 1 - c))

    x_total = dot(nrm[:, 0:512], gx[0].reshape(512, 512))
    y_total = dot(nrm[:, 0:512], gy[0].reshape(512, 512))
    for k in range(1, 4):
        x_total += dot(nrm[:, 512 * k:512 * k + 512], gx[k].reshape(512, 512))
        y_total += dot(nrm[:, 512 * k:512 * k + 512], gy[k].reshape(512, 512))
    x_proj = x_total.astype(BF16)
    x_out[...] = x_proj
    conv_out = (csum[...] + x_proj.astype(F32) * taps[3:4, :]).astype(BF16)
    load(7).wait()
    for p in range(4):
        lanes = slice(128 * p, 128 * p + 128)
        co = conv_out[:, lanes]
        gate_in = sigmoid(dot(co, bd_in[p]))
        gate_dec = sigmoid(dot(co, bd_dec[p]))
        log_sig = -jnp.log(1.0 + jnp.exp(-decay_param[:, lanes]))
        log_decay = decay_scale * gate_dec * log_sig
        inject = jnp.sqrt(neg_expm1(2.0 * log_decay))
        state = jnp.exp(log_decay) * lru[:, lanes] + inject * gate_in * co.astype(F32)
        new_lru[:, lanes] = state
        yv = y_total[:, lanes].astype(BF16).astype(F32)
        gout[:, lanes] = (state * jax.nn.gelu(yv, approximate=True)).astype(BF16)

    load(8).wait()
    for k in range(4):
        lanes = slice(512 * k, 512 * k + 512)
        pp[:, :, lanes] = dot(gout[...], wo[:, lanes]).reshape(4, 16, 512).astype(BF16)

    def rs(k):
        to = m4(x + k)
        return cp(pp.at[to], rsb.at[x], rs_s.at[k], rs_r.at[k], (ep, to))

    for k in (2, 1, 3):
        go(rs(k))

    for a in range(2):
        lo, hi, r = m4(x - 1), m4(x + 1), wrows[a]
        w_got(a, 0, wdst[a].at[c, lo])
        part = wdst[a].at[c, lo, pl.ds(0, r), :]
        w_go(a, 2, part, part, (ep, hi))
        w_go(a, 5, wdst[a].at[c, lo], wdst[a].at[c, lo], (chip * 2 + 1 - c, x))
        w_got(a, 1, wdst[a].at[c, hi])
        part = wdst[a].at[c, hi, pl.ds(r, r), :]
        w_go(a, 3, part, part, (ep, lo))
        w_go(a, 6, wdst[a].at[c, hi], wdst[a].at[c, hi], (chip * 2 + 1 - c, x))

    mixed = pp[x].astype(F32)
    for k in (1, 3, 2):
        frm = m4(x - k)
        cp(rsb.at[frm], rsb.at[frm], rs_s.at[k], rs_r.at[k], (ep, frm)).wait_recv()
        mixed += rsb[frm].astype(F32)
    summed = (hid[pl.ds(pl.multiple_of(16 * x, 16), 16), :].astype(F32) + mixed).astype(BF16)
    for k in range(4):
        smb[k] = summed[:, 512 * k:512 * k + 512]
    xall[x] = rms_scale(summed.astype(F32), ffn_gain[...]).astype(BF16)
    dtok[chip] = xall[x]

    for k in (2, 1, 3):
        to = m4(x + k)
        go(cp(xall.at[x], xall.at[x], xa_s.at[k], xa_r.at[k], (ep, to)))

    def tok(k):
        to = lax.rem(chip + k, 16)
        return cp(xall.at[x], dtok.at[chip], da_s.at[k], da_r.at[k], (to * 2 + c, x))

    def each(first_k, end_k, act):
        def step(k, carry):
            act(k)
            return carry
        lax.fori_loop(first_k, end_k, step, 0)

    each(1, 16, lambda k: tok(k).start())
    for k in (2, 1, 3):
        to = m4(x + k)
        go(cp(smb.at[to], sxb.at[x], sm_s.at[k], sm_r.at[k], (ep, to)))
    sxb[x] = smb[x]

    for k in (1, 3, 2):
        frm = m4(x - k)
        cp(xall.at[frm], xall.at[frm], xa_s.at[k], xa_r.at[k], (ep, frm)).wait_recv()
    for k in range(8):
        fstack[64 * k:64 * k + 64, :] = xall[:, :, 256 * k:256 * k + 256].reshape(64, 256)
    for k in range(4):
        part = slice(384 * k, 384 * k + 384)
        disp[8 * k:8 * k + 8] = dot(sel[part, :], fstack[...]).reshape(8, 48, 256).astype(BF16)
    arr[ep] = disp[ep]

    def route(k):
        to = lax.rem(ep + k, 32)
        return cp(disp.at[to], arr.at[ep], di_s.at[k], di_r.at[k], (to, x))

    each(1, 32, lambda k: route(k).start())

    for a in range(2):
        far = m4(x + 2)
        r = wrows[a]
        w_got(a, 2, wdst[a].at[c, far, pl.ds(0, r), :])
        w_got(a, 3, wdst[a].at[c, far, pl.ds(r, r), :])
        w_go(a, 7, wdst[a].at[c, far], wdst[a].at[c, far], (chip * 2 + 1 - c, x))
    for a in range(2):
        for idx, off in ((4, 0), (5, -1), (6, 1), (7, 2)):
            w_got(a, idx, wdst[a].at[1 - c, m4(x + off)])

    def tok_got(k):
        frm = lax.rem(chip + 16 - k, 16)
        cp(dtok.at[frm], dtok.at[frm], da_s.at[k], da_r.at[k], (frm * 2 + c, x)).wait_recv()

    each(1, 16, tok_got)
    for cc in range(2):
        gu = dot(dtok[:, :, 0:512].reshape(256, 512), wgu[cc, 0])
        for k in range(1, 4):
            gu += dot(dtok[:, :, 512 * k:512 * k + 512].reshape(256, 512), wgu[cc, k])
        g0, u0, t2 = gu[:, 0:128], gu[:, 128:256], gu[:, 256:384]
        dhid[cc, :, 0:128] = (g0 * sigmoid(g0) * u0).astype(BF16)
        dhid[cc, :, 128:256] = (t2 * sigmoid(t2) * pltpu.roll(t2, 64, 1)).astype(BF16)
    for k in range(4):
        out = dot(dhid[0, :, 0:192], wd[0, k]) + dot(dhid[1, :, 0:192], wd[1, k])
        dpart[:, :, 512 * k:512 * k + 512] = out.reshape(16, 16, 512).astype(BF16)

    def dred(k):
        to = lax.rem(chip + k, 16)
        return cp(dpart.at[to], drecv.at[chip], dr_s.at[k], dr_r.at[k], (to * 2 + c, x))

    each(1, 16, lambda k: dred(k).start())
    drecv[chip] = dpart[chip]

    def route_got(k):
        frm = lax.rem(ep + 32 - k, 32)
        cp(arr.at[frm], arr.at[frm], di_s.at[k], di_r.at[k], (frm, x)).wait_recv()

    each(1, 32, route_got)
    for k in range(4):
        moved = dot(perm[...], arr[8 * k:8 * k + 8].reshape(384, 256)).astype(BF16)
        for j in range(8):
            xrows[48 * k:48 * k + 48, 256 * j:256 * j + 256] = moved[48 * j:48 * j + 48, :]
    load(9).wait()
    load(10).wait()
    for k in range(3):
        lanes = slice(256 * k, 256 * k + 256)
        gv = dot(xrows[...], eg[:, lanes])
        uv = dot(xrows[...], eu[:, lanes])
        inner[:, lanes] = (gv * sigmoid(gv) * uv).astype(BF16)
    load(11).wait()
    for k in (2, 1, 3, 0):
        to = m4(x + k)
        pe[to] = dot(inner[...], ed[:, pl.ds(pl.multiple_of(512 * to, 512), 512)]).astype(BF16)
        if k:
            go(cp(pe.at[to], er.at[x], er_s.at[k], er_r.at[k], (ep, to)))

    def dred_got(k):
        frm = lax.rem(chip + 16 - k, 16)
        cp(drecv.at[frm], drecv.at[frm], dr_s.at[k], dr_r.at[k], (frm * 2 + c, x)).wait_recv()

    each(1, 16, dred_got)
    for k in range(4):
        dsb[k] = jnp.sum(drecv[:, :, 512 * k:512 * k + 512].astype(F32), axis=0).astype(BF16)
    for k in (2, 1, 3):
        to = m4(x + k)
        go(cp(dsb.at[to], dxb.at[x], dx_s.at[k], dx_r.at[k], (ep, to)))
    dxb[x] = dsb[x]

    total = pe[x].astype(F32)
    for k in (1, 3, 2):
        frm = m4(x - k)
        cp(er.at[frm], er.at[frm], er_s.at[k], er_r.at[k], (ep, frm)).wait_recv()
        total += er[frm].astype(F32)
    total = total.astype(BF16)
    ret[...] = (
        dot(qmat[:, 0:192], total[:, 0:256]) + dot(qmat[:, 192:384], total[:, 256:512])
    ).reshape(32, 16, 256).astype(BF16)
    back[ep] = ret[ep]

    def giveback(k):
        to = lax.rem(ep + k, 32)
        return cp(ret.at[to], back.at[ep], re_s.at[k], re_r.at[k], (to, x))

    each(1, 32, lambda k: giveback(k).start())

    for k in (1, 3, 2):
        frm = m4(x - k)
        cp(sxb.at[frm], sxb.at[frm], sm_s.at[k], sm_r.at[k], (ep, frm)).wait_recv()
        cp(dxb.at[frm], dxb.at[frm], dx_s.at[k], dx_r.at[k], (ep, frm)).wait_recv()
    share = sigmoid(branch_gate[...])
    rest = sxb[...].reshape(64, 512).astype(F32) + share * dxb[...].reshape(64, 512).astype(F32)

    def back_got(k):
        frm = lax.rem(ep + 32 - k, 32)
        cp(back.at[frm], back.at[frm], re_s.at[k], re_r.at[k], (frm, x)).wait_recv()

    each(1, 32, back_got)
    rows_back = back[...].reshape(512, 256)
    for j in range(2):
        lanes = slice(256 * j, 256 * j + 256)
        esum = dot(comb[j, 0], rows_back) + dot(comb[j, 1], rows_back)
        new_hidden[:, lanes] = (rest[:, lanes] + esum).astype(BF16)

    for copy in sent:
        copy.wait_send()
    each(1, 16, lambda k: tok(k).wait_send())
    each(1, 16, lambda k: dred(k).wait_send())
    each(1, 32, lambda k: route(k).wait_send())
    each(1, 32, lambda k: giveback(k).wait_send())


def on_device(
    hidden, mix_gain, proj_x, proj_y, conv_taps, input_gate, decay_gate, decay_param, proj_out,
    conv_state, lru_state, ffn_gain, routes, route_weights, expert_gate, expert_up, expert_down,
    dense_gate, dense_up, dense_down, branch_gate,
):
    vmem = pl.BlockSpec(memory_space=pltpu.VMEM)
    hbm = pl.BlockSpec(memory_space=pl.ANY)
    V = pltpu.VMEM
    dma = pltpu.SemaphoreType.DMA
    scratch = [
        V((64, D), BF16), V((64, COLS), BF16), V((64, COLS), BF16), V((COLS, D), BF16),
        V((64, 3, COLS), BF16), V((64, COLS), F32), V((D, 768), BF16), V((D, 768), BF16),
        V((768, D), BF16), V((COLS, 192), BF16), V((COLS, 192), BF16), V((192, COLS), BF16),
        V((4, 4, 2, 64, COLS), BF16), V((4, 4, 2, 64, COLS), BF16), V((COLS, 384), BF16),
        V((2, 4, COLS, 384), BF16), V((2, 4, 192, COLS), BF16), V((64, D), BF16),
        V((4, 128, 128), BF16), V((4, 128, 128), BF16), V((64, COLS), F32), V((64, COLS), BF16),
        V((4, 16, D), BF16), V((4, 16, D), BF16), V((4, 16, COLS), BF16), V((4, 16, COLS), BF16),
        V((4, 16, D), BF16), V((16, 16, D), BF16),
        V((512, 256), BF16), V((1536, 512), BF16), V((2, 2, 64, 512), BF16), V((384, 384), BF16),
        V((512, 384), BF16), V((32, 48, 256), BF16), V((32, 48, 256), BF16), V((192, D), BF16),
        V((192, 768), BF16), V((4, 192, COLS), BF16), V((4, 192, COLS), BF16),
        V((32, 16, 256), BF16), V((32, 16, 256), BF16),
        V((2, 256, 256), BF16), V((16, 16, D), BF16), V((16, 16, D), BF16),
        V((4, 16, COLS), BF16), V((4, 16, COLS), BF16),
        dma((12,)), dma((2, 36)), dma((2, 36)), dma((2, 8)), dma((2, 8)), dma((4,)), dma((4,)),
        dma((4,)), dma((4,)), dma((4,)), dma((4,)), dma((16,)), dma((16,)), dma((32,)), dma((32,)),
        dma((4,)), dma((4,)), dma((32,)), dma((32,)), dma((16,)), dma((16,)), dma((4,)), dma((4,)),
    ]
    new_hidden, new_lru, x_proj = pl.pallas_call(
        kernel,
        out_shape=(
            jax.ShapeDtypeStruct((64, COLS), BF16),
            jax.ShapeDtypeStruct((64, COLS), F32),
            jax.ShapeDtypeStruct((64, COLS), BF16),
        ),
        in_specs=[vmem] * 9 + [hbm] * 12,
        out_specs=(vmem, vmem, vmem),
        scratch_shapes=scratch,
        compiler_params=pltpu.CompilerParams(
            collective_id=0, has_side_effects=True, vmem_limit_bytes=58 * 1024 * 1024
        ),
        name="decode_layer",
    )(
        mix_gain.reshape(1, D), conv_taps, input_gate, decay_gate, decay_param.reshape(1, COLS),
        ffn_gain.reshape(1, D), routes, route_weights, branch_gate.reshape(1, COLS),
        hidden, proj_x, proj_y, proj_out, conv_state, lru_state, expert_gate, expert_up,
        expert_down, dense_gate, dense_up, dense_down,
    )
    new_conv = jnp.concatenate([conv_state[:, 1:], x_proj[:, None, :]], axis=1)
    return (new_hidden, new_lru, new_conv)


def solution(mesh):
    in_specs = (
        P("ep", None), P(), P("ep", "tp"), P("ep", "tp"), P(None, "tp"), P("tp", None, None),
        P("tp", None, None), P("tp"), P("tp", None), P("ep", None, "tp"), P("ep", "tp"), P(),
        P("ep", None), P("ep", None), P("ep", None, "tp"), P("ep", None, "tp"),
        P("ep", "tp", None), P("tp", "ep"), P("tp", "ep"), P("ep", "tp"), P("tp"),
    )
    out_specs = (P("ep", "tp"), P("ep", "tp"), P("ep", None, "tp"))
    return jax.shard_map(
        on_device, mesh=mesh, in_specs=in_specs, out_specs=out_specs, check_vma=False
    )
```

time: 279 us -> 106 us (0.38)
  waiting for transfers between devices: 125 us -> 0 us
  Pallas kernels: 0 us -> 89.9 us
  blocking collectives: 60.9 us -> 0 us
  matrix products: 26.5 us -> 0 us
  starting transfers between devices: 16.7 us -> 0 us
  between operations: 14 us -> 0.65 us
  other arithmetic: 14.7 us -> 1.54 us
  local copies, waits for them, and re-layouts: 19.7 us -> 13.7 us
    pallas_call x0 -> x1, Pallas kernels: none -> 89.9 us  [on_device(): pl.pallas_call(kernel, out_shape=(jax.ShapeDtypeStruct((64, COLS), BF16),...]
    all_to_all x2 -> x0, blocking collectives: 60.9 us -> none  [the longest x1 36.1 us: copy_for_each(): return lax.all_to_all(copies, axis, split_axis=0, concat_axis=0, tiled=True)]
    all_gather x1 -> x0, waiting for transfers between devices: 48.5 us -> none  [in_one_piece(): whole = lax.all_gather(both, axis, axis=dim, tiled=True)]
    psum x1 -> x0, waiting for transfers between devices: 45.7 us -> none  [on_device(): lax.psum(dense_part.astype(jnp.bfloat16), 'tp').astype(jnp.float32)]
    all_to_all x4 -> x0, waiting for transfers between devices: 30.8 us -> none  [the longest x2 17.8 us: sum_at_owner(): lax.all_to_all(split_up(value, dim, devices), axis, 0, 0, tiled=True)]
    dot_general x10 -> x0, matrix products: 26.5 us -> none  [the longest x1 5.15 us: on_device(): jnp.einsum('sgif,gfd->sgid', inner_act, expert_down, preferred_element_ty...]
    all_to_all x4 -> x0, starting transfers between devices: 16.6 us -> none  [the longest x2 8.36 us: sum_at_owner(): lax.all_to_all(split_up(value, dim, devices), axis, 0, 0, tiled=True)]
    unnamed x27 -> x7, local copies, waits for them, and re-layouts: 2.23 us -> 11.1 us
  transfers between devices with their start and end apart: 7 -> 0, of which waited for: 6 -> 0; matrix products, arithmetic and copies ran while one was open for 11% -> 0% of each run, Pallas kernels for 0% -> 0%
where the time goes in v1:
time: 106 us
  Pallas kernels  89.9 us (85%)
  local copies, waits for them, and re-layouts  13.7 us (13%)
  other arithmetic  1.54 us (1%)
    pallas_call x1, Pallas kernels, on_device(): pl.pallas_call(kernel, out_shape=(jax.ShapeDtypeStruct((64, COLS), BF16),...  89.9 us
    unnamed x7, local copies, waits for them, and re-layouts  11.1 us

profile of v1, /device:TPU:1, one launch (start us, length us, event | category | flops | bytes accessed | tf_op | source)
XLA Modules:
  0.0 105.8 jit_solution(8737965105802159833)
XLA Ops:
  0.6 1.8 %copy.26.conv_h = bf16[64,3,512]{2,1,0:T(4,128)(2,1)} copy(bf16[64,3,512]{2,0,1:T(8,128)(2,1)} %param.30) | data formatting | bytes 393216 | tf_op args[9]
  2.4 1.8 %copy.27.dg_h = bf16[512,192]{1,0:T(8,128)(2,1)} copy(bf16[512,192]{0,1:T(8,128)(2,1)} %param.38) | data formatting | bytes 393216 | tf_op args[17]
  4.2 1.8 %copy.28.du_h = bf16[512,192]{1,0:T(8,128)(2,1)} copy(bf16[512,192]{0,1:T(8,128)(2,1)} %param.39) | data formatting | bytes 393216 | tf_op args[18]
  5.9 1.4 %copy.24.routes = s32[64,2]{1,0:T(8,128)} copy(s32[64,2]{0,1:T(2,128)} %param.33) | data formatting | bytes 1024 | tf_op args[12]
  7.3 1.4 %copy.25.route_weights = f32[64,2]{1,0:T(8,128)} copy(f32[64,2]{0,1:T(2,128)} %param.34) | data formatting | bytes 1024 | tf_op args[13]
  8.7 1.3 %reshape.18.mix_gain = bf16[1,2048]{1,0:T(2,128)(2,1)} reshape(bf16[2048]{0:T(1024)(128)(2,1)} %param.22) | data formatting | bytes 8192 | tf_op jit(solution)/shard_map/reshape | solution.py:555
  10.0 1.3 %reshape.20.ffn_gain = bf16[1,2048]{1,0:T(2,128)(2,1)} reshape(bf16[2048]{0:T(1024)(128)(2,1)} %param.32) | data formatting | bytes 8192 | tf_op jit(solution)/shard_map/reshape | solution.py:556
  11.3 0.0 slice-start
  11.3 89.9 %decode_layer.1 = (bf16[64,512]{1,0:T(8,128)(2,1)}, f32[64,512]{1,0:T(8,128)}, bf16[64,512]{1,0:T(8,128)(2,1)}) custom-call(bf16[1,2048]{1,0:T(2,128)(2,1)} %reshape.18.mix_gain, bf16[4,512]{1,0:T(4,128)(2,1)} %conv_taps.1, bf16[8,64,64]{2,1,0:T(8,128)(2,1)} %input_gate.1, bf16[8,64,64]{2,1,0:T(8,128)(2,1)} %decay_gate.1, f32[1,512]{1,0:T(1,128)} %bitcast.4, ...), custom_call_target="tpu_custom_call" | custom-call | tf_op jit(solution)/shard_map/decode_layer/pallas_call | solution.py:540
  101.2 0.0 slice-done
  101.2 1.5 %pad_maximum_fusion = bf16[64,3,512]{2,0,1:T(8,128)(2,1)} fusion(bf16[64,1,512]{2,0,1:T(8,128)(2,1)} %bitcast.3, bf16[64,2,512]{2,0,1:T(8,128)(2,1)S(1)} %slice-done), kind=kLoop, calls=%fused_computation | loop fusion | flops 98304 | bytes 393216 | tf_op jit(solution)/shard_map/concatenate | solution.py:560
  102.8 1.5 %copy.31 = bf16[64,512]{1,0:T(8,128)(2,1)} copy(bf16[64,512]{1,0:T(8,128)(2,1)} %get-tuple-element.12) | data formatting | bytes 131072
  104.2 1.6 %copy.32 = f32[64,512]{1,0:T(8,128)} copy(f32[64,512]{1,0:T(8,128)} %get-tuple-element.13) | data formatting | bytes 262144
Async XLA Ops:
  11.3 89.9 %slice-start = ((bf16[64,3,512]{2,0,1:T(8,128)(2,1)}), bf16[64,2,512]{2,0,1:T(8,128)(2,1)S(1)}, s32[]{:S(2)}) async-start(bf16[64,3,512]{2,0,1:T(8,128)(2,1)} %param.30), calls=%async_computation | async-start | bytes 262144 | tf_op jit(solution)/shard_map/slice | solution.py:560

commit v2 on v1

--- a/solution.py
+++ b/solution.py
@@ -38,8 +38,11 @@
 
 
 def rms_scale(floats, gain):
-    meansq = jnp.mean(floats * floats, axis=-1, keepdims=True)
-    return floats * lax.rsqrt(meansq + epsilon) * gain.astype(F32)
+    scale = lax.rsqrt(jnp.mean(floats * floats, axis=-1, keepdims=True) + epsilon)
+    gains = gain[...].astype(F32)
+    return jnp.concatenate(
+        [floats[:, 128 * k:128 * k + 128] * scale * gains[k:k + 1, :] for k in range(16)], axis=1
+    )
 
 
 def sigmoid(v):
@@ -55,9 +58,9 @@
     mix_gain, conv_taps, input_gate, decay_gate, decay_param, ffn_gain, routes, route_weights,
     branch_gate, hidden_h, proj_x_h, proj_y_h, proj_out_h, conv_h, lru_h, eg_h, eu_h, ed_h,
     dg_h, du_h, dd_h,
-    new_hidden, new_lru, x_out,
-    hid, px, py, wo, conv, lru, eg, eu, ed, dg, du, dd,
-    gx, gy, wown, wgu, wd, nrm, bd_in, bd_dec, csum, gout, pp, rsb, smb, sxb, xall, dtok,
+    new_hidden, new_lru, new_conv,
+    hid, px, py, wo, conv, lru, eg, eu, ed, dgu, dd,
+    gx, gy, wgu, wd, nrm, bd_in, bd_dec, csum, gout, pp, rsb, smb, sxb, xall, dtok,
     fstack, sel, comb, perm, qmat, disp, arr, xrows, inner, pe, er, ret, back,
     dhid, dpart, drecv, dsb, dxb,
     lsem, ag_s, ag_r, dw_s, dw_r, rs_s, rs_r, xa_s, xa_r, sm_s, sm_r, da_s, da_r,
@@ -78,8 +81,17 @@
             src_ref=src, dst_ref=dst, send_sem=ssem, recv_sem=rsem, device_id=dev, device_id_type=MESH
         )
 
+    scopes = []
+
+    def phase(name):
+        if scopes:
+            scopes.pop().__exit__(None, None, None)
+        if name:
+            scopes.append(jax.named_scope(name))
+            scopes[-1].__enter__()
+
     loads = [
-        (proj_x_h, px), (proj_y_h, py), (hidden_h, hid), (dg_h, dg), (du_h, du), (dd_h, dd),
+        (proj_x_h, px), (proj_y_h, py), (hidden_h, hid), (dg_h, dgu.at[0]), (du_h, dgu.at[1]), (dd_h, dd),
         (conv_h, conv), (lru_h, lru), (proj_out_h, wo), (eg_h.at[0], eg), (eu_h.at[0], eu),
         (ed_h.at[0], ed),
     ]
@@ -87,6 +99,7 @@
     def load(k):
         return pltpu.make_async_copy(loads[k][0], loads[k][1], lsem.at[k])
 
+    phase("barrier")
     for k in range(len(loads)):
         load(k).start()
 
@@ -103,6 +116,7 @@
     load(1).wait()
     pl.semaphore_wait(bar, 34)
 
+    phase("ag_start")
     own = (px, py)
     bufs = (gx, gy)
     first = (y, z)
@@ -162,19 +176,12 @@
     c128 = iota((64, 128), 1)
     put = (mask(c128 == r64).astype(BF16), mask(c128 == r64 + 64).astype(BF16))
 
+    phase("dense_w_start")
     load(3).wait()
     load(4).wait()
     load(5).wait()
-    wown[:, 0:128] = dg[:, 0:128]
-    wown[:, 128:256] = du[:, 0:128]
-    wown[:, 256:384] = (dot(dg[:, 128:192], put[0]) + dot(du[:, 128:192], put[1])).astype(BF16)
-
-    load(2).wait()
-    nrm[...] = rms_scale(hid[...].astype(F32), mix_gain[...]).astype(BF16)
-
-    wsrc = (wown, dd)
+    wsrc = (dgu, dd)
     wdst = (wgu, wd)
-    wrows = (256, 96)
 
     def w_go(a, idx, src, dst, device):
         go(cp(src, dst, dw_s.at[a, idx], dw_r.at[a, idx], device))
@@ -186,9 +193,19 @@
         w_go(a, 0, wsrc[a], wdst[a].at[c, x], (ep, m4(x + 1)))
         w_go(a, 1, wsrc[a], wdst[a].at[c, x], (ep, m4(x - 1)))
         w_go(a, 4, wsrc[a], wdst[a].at[c, x], (chip * 2 + 1 - c, x))
-    wgu[c, x] = wown[...]
+    wgu[c, x] = dgu[...]
     wd[c, x] = dd[...]
 
+    def w_half(a, xx, half):
+        if a == 0:
+            return wgu.at[c, xx, half]
+        return wd.at[c, xx, pl.ds(96 * half, 96), :]
+
+    phase("norm")
+    load(2).wait()
+    nrm[...] = rms_scale(hid[...].astype(F32), mix_gain).astype(BF16)
+
+    phase("ag_first")
     for h in range(2):
         f, s = first[h], second[h]
         lo, hi = m4(f - 1), m4(f + 1)
@@ -217,13 +234,15 @@
         got(h, 7 + 4 * i, piece(h, f, s, 1))
         across(h, i, 3)
 
-    e32 = iota((64, 32), 1)
-    oh = [mask(routes[:, r:r + 1] == e32) for r in range(2)]
+    phase("routes")
+    e32 = iota((32, 64), 0)
+    oh = [mask(routes[r:r + 1, :] == e32) for r in range(2)]
     both = oh[0] + oh[1]
-    lower = mask(iota((64, 64), 1) < iota((64, 64), 0)).astype(BF16)
-    rank1 = both * (dot(lower, both.astype(BF16)) + 1.0)
-    rank1b = rank1.astype(BF16)
-
+    upper = mask(iota((64, 64), 0) < iota((64, 64), 1)).astype(BF16)
+    rank1 = (both * (dot(both.astype(BF16), upper) + 1.0)).astype(BF16)
+    eye = mask(iota((64, 64), 0) == iota((64, 64), 1)).astype(BF16)
+
+    phase("ag_a0")
     for h in range(2):
         arrivals(h, 0)
     for h in range(2):
@@ -233,23 +252,30 @@
         second_phase(h, 3, slot(h, f, s, c))
         across(h, 3, 0)
 
+    phase("blockdiag")
     for p in range(4):
         for gate, block in ((input_gate, bd_in), (decay_gate, bd_dec)):
             for k in range(2):
                 block[p, 64 * k:64 * k + 64, :] = dot(gate[2 * p + k], put[k]).astype(BF16)
 
+    phase("ag_a1")
     for h in range(2):
         arrivals(h, 1)
 
+    phase("conv")
     load(6).wait()
     taps = conv_taps[...].astype(F32)
-    csum[...] = jnp.sum(conv[...].astype(F32) * taps[None, 0:3, :], axis=1)
-
+    csum[...] = sum(conv[k].astype(F32) * taps[k:k + 1, :] for k in range(3))
+    new_conv[0] = conv[1]
+    new_conv[1] = conv[2]
+
+    phase("ag_a2")
     for h in range(2):
         arrivals(h, 2)
 
-    tt = mask((iota((512, 64), 0) & 63) == iota((512, 64), 1)).astype(BF16)
-    spread = dot(tt, rank1b).astype(BF16)
+    phase("selmat")
+    tt = mask((iota((64, 512), 1) & 63) == iota((64, 512), 0)).astype(BF16)
+    spread = dot(rank1, tt).astype(BF16)
     rows = iota((1536, 32), 0)
     ecol = iota((1536, 32), 1) * 48
     erow = mask((rows >= ecol) & (rows < ecol + 48)).astype(BF16)
@@ -259,13 +285,15 @@
     ck1 = div6(rin)
     slot1 = (rin - 6 * ck1 + 1).astype(F32)
     ckcol = iota((1536, 512), 1) >> 6
-    sel[...] = mask((dot_nt(erow, spread) == slot1) & (ck1 == ckcol)).astype(BF16)
-
+    sel[...] = mask((dot(erow, spread) == slot1) & (ck1 == ckcol)).astype(BF16)
+
+    phase("ag_l0")
     for h in range(2):
         last(h, 0)
     for h in range(2):
         arrivals(h, 3)
 
+    phase("perms")
     pr = iota((384, 384), 0)
     pc = iota((384, 384), 1)
     prc = div6(pr >> 3)
@@ -277,42 +305,45 @@
     qslot = qr & 7
     qmat[...] = mask((qslot < 6) & (qc == ((qr >> 3) & 1) * 192 + (qr >> 4) * 6 + qslot)).astype(BF16)
 
+    phase("ag_l1")
     for h in range(2):
         last(h, 1)
 
-    w0 = route_weights[:, 0:1]
-    w1 = route_weights[:, 1:2]
-    wfull = w0 * oh[0] + w1 * oh[1]
+    phase("combs")
+    wfull = route_weights[0:1, :] * oh[0] + route_weights[1:2, :] * oh[1]
     whi = wfull.astype(BF16)
     wlo = (wfull - whi.astype(F32)).astype(BF16)
     expand = mask((iota((32, 512), 1) >> 4) == iota((32, 512), 0)).astype(BF16)
     ccol = iota((64, 512), 1)
-    hit = dot(rank1b, expand) == ((ccol & 7) + 1).astype(F32)
-    ehi = dot(whi, expand)
-    elo = dot(wlo, expand)
+    hit = dot(dot_nt(eye, rank1).astype(BF16), expand) == ((ccol & 7) + 1).astype(F32)
+    ehi = dot(dot_nt(eye, whi).astype(BF16), expand)
+    elo = dot(dot_nt(eye, wlo).astype(BF16), expand)
     for j in range(2):
         here = hit & (((ccol >> 3) & 1) == j)
         comb[j, 0] = jnp.where(here, ehi, 0.0).astype(BF16)
         comb[j, 1] = jnp.where(here, elo, 0.0).astype(BF16)
 
+    phase("ag_l2")
     for h in range(2):
         last(h, 2)
     for h in range(2):
         last(h, 3)
 
+    phase("ag_partner")
     for h in range(2):
         for si in range(4):
             for i in range(4):
                 f, s = m4(first[h] + OFFS[i]), m4(second[h] + OFFS[si])
                 got(h, 20 + 4 * si + i, slot(h, f, s, 1 - c))
 
+    phase("proj_lru")
     x_total = dot(nrm[:, 0:512], gx[0].reshape(512, 512))
     y_total = dot(nrm[:, 0:512], gy[0].reshape(512, 512))
     for k in range(1, 4):
         x_total += dot(nrm[:, 512 * k:512 * k + 512], gx[k].reshape(512, 512))
         y_total += dot(nrm[:, 512 * k:512 * k + 512], gy[k].reshape(512, 512))
     x_proj = x_total.astype(BF16)
-    x_out[...] = x_proj
+    new_conv[2] = x_proj
     conv_out = (csum[...] + x_proj.astype(F32) * taps[3:4, :]).astype(BF16)
     load(7).wait()
     for p in range(4):
@@ -328,6 +359,7 @@
         yv = y_total[:, lanes].astype(BF16).astype(F32)
         gout[:, lanes] = (state * jax.nn.gelu(yv, approximate=True)).astype(BF16)
 
+    phase("outproj")
     load(8).wait()
     for k in range(4):
         lanes = slice(512 * k, 512 * k + 512)
@@ -340,17 +372,19 @@
     for k in (2, 1, 3):
         go(rs(k))
 
+    phase("dense_w_relay")
     for a in range(2):
-        lo, hi, r = m4(x - 1), m4(x + 1), wrows[a]
+        lo, hi = m4(x - 1), m4(x + 1)
         w_got(a, 0, wdst[a].at[c, lo])
-        part = wdst[a].at[c, lo, pl.ds(0, r), :]
+        part = w_half(a, lo, 0)
         w_go(a, 2, part, part, (ep, hi))
         w_go(a, 5, wdst[a].at[c, lo], wdst[a].at[c, lo], (chip * 2 + 1 - c, x))
         w_got(a, 1, wdst[a].at[c, hi])
-        part = wdst[a].at[c, hi, pl.ds(r, r), :]
+        part = w_half(a, hi, 1)
         w_go(a, 3, part, part, (ep, lo))
         w_go(a, 6, wdst[a].at[c, hi], wdst[a].at[c, hi], (chip * 2 + 1 - c, x))
 
+    phase("rs_wait")
     mixed = pp[x].astype(F32)
     for k in (1, 3, 2):
         frm = m4(x - k)
@@ -359,9 +393,10 @@
     summed = (hid[pl.ds(pl.multiple_of(16 * x, 16), 16), :].astype(F32) + mixed).astype(BF16)
     for k in range(4):
         smb[k] = summed[:, 512 * k:512 * k + 512]
-    xall[x] = rms_scale(summed.astype(F32), ffn_gain[...]).astype(BF16)
+    xall[x] = rms_scale(summed.astype(F32), ffn_gain).astype(BF16)
     dtok[chip] = xall[x]
 
+    phase("ffn_send")
     for k in (2, 1, 3):
         to = m4(x + k)
         go(cp(xall.at[x], xall.at[x], xa_s.at[k], xa_r.at[k], (ep, to)))
@@ -382,9 +417,11 @@
         go(cp(smb.at[to], sxb.at[x], sm_s.at[k], sm_r.at[k], (ep, to)))
     sxb[x] = smb[x]
 
+    phase("xag_wait")
     for k in (1, 3, 2):
         frm = m4(x - k)
         cp(xall.at[frm], xall.at[frm], xa_s.at[k], xa_r.at[k], (ep, frm)).wait_recv()
+    phase("dispatch")
     for k in range(8):
         fstack[64 * k:64 * k + 64, :] = xall[:, :, 256 * k:256 * k + 256].reshape(64, 256)
     for k in range(4):
@@ -398,11 +435,11 @@
 
     each(1, 32, lambda k: route(k).start())
 
+    phase("dense_w_wait")
     for a in range(2):
         far = m4(x + 2)
-        r = wrows[a]
-        w_got(a, 2, wdst[a].at[c, far, pl.ds(0, r), :])
-        w_got(a, 3, wdst[a].at[c, far, pl.ds(r, r), :])
+        w_got(a, 2, w_half(a, far, 0))
+        w_got(a, 3, w_half(a, far, 1))
         w_go(a, 7, wdst[a].at[c, far], wdst[a].at[c, far], (chip * 2 + 1 - c, x))
     for a in range(2):
         for idx, off in ((4, 0), (5, -1), (6, 1), (7, 2)):
@@ -412,16 +449,20 @@
         frm = lax.rem(chip + 16 - k, 16)
         cp(dtok.at[frm], dtok.at[frm], da_s.at[k], da_r.at[k], (frm * 2 + c, x)).wait_recv()
 
+    phase("dense_tok_wait")
     each(1, 16, tok_got)
+    phase("dense_gu")
     for cc in range(2):
-        gu = dot(dtok[:, :, 0:512].reshape(256, 512), wgu[cc, 0])
-        for k in range(1, 4):
-            gu += dot(dtok[:, :, 512 * k:512 * k + 512].reshape(256, 512), wgu[cc, k])
-        g0, u0, t2 = gu[:, 0:128], gu[:, 128:256], gu[:, 256:384]
-        dhid[cc, :, 0:128] = (g0 * sigmoid(g0) * u0).astype(BF16)
-        dhid[cc, :, 128:256] = (t2 * sigmoid(t2) * pltpu.roll(t2, 64, 1)).astype(BF16)
+        gv = jnp.zeros((256, 192), F32)
+        uv = jnp.zeros((256, 192), F32)
+        for k in range(4):
+            part = dtok[:, :, 512 * k:512 * k + 512].reshape(256, 512)
+            gv += dot_nt(part, wgu[cc, k, 0])
+            uv += dot_nt(part, wgu[cc, k, 1])
+        dhid[cc] = (gv * sigmoid(gv) * uv).astype(BF16)
+    phase("dense_down")
     for k in range(4):
-        out = dot(dhid[0, :, 0:192], wd[0, k]) + dot(dhid[1, :, 0:192], wd[1, k])
+        out = dot(dhid[0], wd[0, k]) + dot(dhid[1], wd[1, k])
         dpart[:, :, 512 * k:512 * k + 512] = out.reshape(16, 16, 512).astype(BF16)
 
     def dred(k):
@@ -435,11 +476,14 @@
         frm = lax.rem(ep + 32 - k, 32)
         cp(arr.at[frm], arr.at[frm], di_s.at[k], di_r.at[k], (frm, x)).wait_recv()
 
+    phase("dispatch_wait")
     each(1, 32, route_got)
+    phase("perm_rows")
     for k in range(4):
         moved = dot(perm[...], arr[8 * k:8 * k + 8].reshape(384, 256)).astype(BF16)
         for j in range(8):
             xrows[48 * k:48 * k + 48, 256 * j:256 * j + 256] = moved[48 * j:48 * j + 48, :]
+    phase("expert_gu")
     load(9).wait()
     load(10).wait()
     for k in range(3):
@@ -447,6 +491,7 @@
         gv = dot(xrows[...], eg[:, lanes])
         uv = dot(xrows[...], eu[:, lanes])
         inner[:, lanes] = (gv * sigmoid(gv) * uv).astype(BF16)
+    phase("expert_down")
     load(11).wait()
     for k in (2, 1, 3, 0):
         to = m4(x + k)
@@ -458,7 +503,9 @@
         frm = lax.rem(chip + 16 - k, 16)
         cp(drecv.at[frm], drecv.at[frm], dr_s.at[k], dr_r.at[k], (frm * 2 + c, x)).wait_recv()
 
+    phase("dense_red_wait")
     each(1, 16, dred_got)
+    phase("dense_sum")
     for k in range(4):
         dsb[k] = jnp.sum(drecv[:, :, 512 * k:512 * k + 512].astype(F32), axis=0).astype(BF16)
     for k in (2, 1, 3):
@@ -466,11 +513,13 @@
         go(cp(dsb.at[to], dxb.at[x], dx_s.at[k], dx_r.at[k], (ep, to)))
     dxb[x] = dsb[x]
 
+    phase("er_wait")
     total = pe[x].astype(F32)
     for k in (1, 3, 2):
         frm = m4(x - k)
         cp(er.at[frm], er.at[frm], er_s.at[k], er_r.at[k], (ep, frm)).wait_recv()
         total += er[frm].astype(F32)
+    phase("ret_build")
     total = total.astype(BF16)
     ret[...] = (
         dot(qmat[:, 0:192], total[:, 0:256]) + dot(qmat[:, 192:384], total[:, 256:512])
@@ -483,10 +532,12 @@
 
     each(1, 32, lambda k: giveback(k).start())
 
+    phase("rest_wait")
     for k in (1, 3, 2):
         frm = m4(x - k)
         cp(sxb.at[frm], sxb.at[frm], sm_s.at[k], sm_r.at[k], (ep, frm)).wait_recv()
         cp(dxb.at[frm], dxb.at[frm], dx_s.at[k], dx_r.at[k], (ep, frm)).wait_recv()
+    phase("rest")
     share = sigmoid(branch_gate[...])
     rest = sxb[...].reshape(64, 512).astype(F32) + share * dxb[...].reshape(64, 512).astype(F32)
 
@@ -494,19 +545,29 @@
         frm = lax.rem(ep + 32 - k, 32)
         cp(back.at[frm], back.at[frm], re_s.at[k], re_r.at[k], (frm, x)).wait_recv()
 
+    phase("back_wait")
     each(1, 32, back_got)
+    phase("combine")
     rows_back = back[...].reshape(512, 256)
     for j in range(2):
         lanes = slice(256 * j, 256 * j + 256)
         esum = dot(comb[j, 0], rows_back) + dot(comb[j, 1], rows_back)
         new_hidden[:, lanes] = (rest[:, lanes] + esum).astype(BF16)
 
+    phase("send_wait")
     for copy in sent:
         copy.wait_send()
     each(1, 16, lambda k: tok(k).wait_send())
     each(1, 16, lambda k: dred(k).wait_send())
     each(1, 32, lambda k: route(k).wait_send())
     each(1, 32, lambda k: giveback(k).wait_send())
+    phase(None)
+
+
+def publish(a, b, c, a_out, b_out, c_out):
+    a_out[...] = a[...]
+    b_out[...] = b[...]
+    c_out[...] = c[...]
 
 
 def on_device(
@@ -520,10 +581,10 @@
     dma = pltpu.SemaphoreType.DMA
     scratch = [
         V((64, D), BF16), V((64, COLS), BF16), V((64, COLS), BF16), V((COLS, D), BF16),
-        V((64, 3, COLS), BF16), V((64, COLS), F32), V((D, 768), BF16), V((D, 768), BF16),
-        V((768, D), BF16), V((COLS, 192), BF16), V((COLS, 192), BF16), V((192, COLS), BF16),
-        V((4, 4, 2, 64, COLS), BF16), V((4, 4, 2, 64, COLS), BF16), V((COLS, 384), BF16),
-        V((2, 4, COLS, 384), BF16), V((2, 4, 192, COLS), BF16), V((64, D), BF16),
+        V((3, 64, COLS), BF16), V((64, COLS), F32), V((D, 768), BF16), V((D, 768), BF16),
+        V((768, D), BF16), V((2, 192, COLS), BF16), V((192, COLS), BF16),
+        V((4, 4, 2, 64, COLS), BF16), V((4, 4, 2, 64, COLS), BF16),
+        V((2, 4, 2, 192, COLS), BF16), V((2, 4, 192, COLS), BF16), V((64, D), BF16),
         V((4, 128, 128), BF16), V((4, 128, 128), BF16), V((64, COLS), F32), V((64, COLS), BF16),
         V((4, 16, D), BF16), V((4, 16, D), BF16), V((4, 16, COLS), BF16), V((4, 16, COLS), BF16),
         V((4, 16, D), BF16), V((16, 16, D), BF16),
@@ -531,19 +592,20 @@
         V((512, 384), BF16), V((32, 48, 256), BF16), V((32, 48, 256), BF16), V((192, D), BF16),
         V((192, 768), BF16), V((4, 192, COLS), BF16), V((4, 192, COLS), BF16),
         V((32, 16, 256), BF16), V((32, 16, 256), BF16),
-        V((2, 256, 256), BF16), V((16, 16, D), BF16), V((16, 16, D), BF16),
+        V((2, 256, 192), BF16), V((16, 16, D), BF16), V((16, 16, D), BF16),
         V((4, 16, COLS), BF16), V((4, 16, COLS), BF16),
         dma((12,)), dma((2, 36)), dma((2, 36)), dma((2, 8)), dma((2, 8)), dma((4,)), dma((4,)),
         dma((4,)), dma((4,)), dma((4,)), dma((4,)), dma((16,)), dma((16,)), dma((32,)), dma((32,)),
         dma((4,)), dma((4,)), dma((32,)), dma((32,)), dma((16,)), dma((16,)), dma((4,)), dma((4,)),
     ]
-    new_hidden, new_lru, x_proj = pl.pallas_call(
+    shapes = (
+        jax.ShapeDtypeStruct((64, COLS), BF16),
+        jax.ShapeDtypeStruct((64, COLS), F32),
+        jax.ShapeDtypeStruct((3, 64, COLS), BF16),
+    )
+    outs = pl.pallas_call(
         kernel,
-        out_shape=(
-            jax.ShapeDtypeStruct((64, COLS), BF16),
-            jax.ShapeDtypeStruct((64, COLS), F32),
-            jax.ShapeDtypeStruct((64, COLS), BF16),
-        ),
+        out_shape=shapes,
         in_specs=[vmem] * 9 + [hbm] * 12,
         out_specs=(vmem, vmem, vmem),
         scratch_shapes=scratch,
@@ -552,13 +614,19 @@
         ),
         name="decode_layer",
     )(
-        mix_gain.reshape(1, D), conv_taps, input_gate, decay_gate, decay_param.reshape(1, COLS),
-        ffn_gain.reshape(1, D), routes, route_weights, branch_gate.reshape(1, COLS),
-        hidden, proj_x, proj_y, proj_out, conv_state, lru_state, expert_gate, expert_up,
-        expert_down, dense_gate, dense_up, dense_down,
+        mix_gain.reshape(16, 128), conv_taps, input_gate, decay_gate, decay_param.reshape(1, COLS),
+        ffn_gain.reshape(16, 128), routes.T, route_weights.T, branch_gate.reshape(1, COLS),
+        hidden, proj_x, proj_y, proj_out, conv_state.transpose(1, 0, 2), lru_state, expert_gate, expert_up,
+        expert_down, dense_gate.T, dense_up.T, dense_down,
     )
-    new_conv = jnp.concatenate([conv_state[:, 1:], x_proj[:, None, :]], axis=1)
-    return (new_hidden, new_lru, new_conv)
+    new_hidden, new_lru, new_conv = pl.pallas_call(
+        publish,
+        out_shape=shapes,
+        in_specs=[vmem] * 3,
+        out_specs=(vmem,) * 3,
+        name="publish",
+    )(*outs)
+    return (new_hidden, new_lru, new_conv.transpose(1, 0, 2))
 
 
 def solution(mesh):

time: 106 us -> 92.6 us (0.87)
  local copies, waits for them, and re-layouts: 13.7 us -> 0 us
  Pallas kernels: 89.9 us -> 91.8 us
  other arithmetic: 1.54 us -> 0 us
    unnamed x7 -> x0, local copies, waits for them, and re-layouts: 11.1 us -> none
    reshape x2 -> x0, local copies, waits for them, and re-layouts: 2.58 us -> none  [the longest x1 1.29 us: on_device(): mix_gain.reshape(1, D)]
    pallas_call x1 -> x2, Pallas kernels: 89.9 us -> 91.8 us  [the longest x1 90 us: on_device(): pl.pallas_call(kernel, out_shape=shapes, in_specs=[vmem] * 9 + [hbm] * 12...]
    concatenate x1 -> x0, other arithmetic: 1.54 us -> none  [on_device(): new_conv = jnp.concatenate([conv_state[:, 1:], x_proj[:, None, :]], axis=1)]
where the time goes in v2:
time: 92.6 us; the launch traced here: 92.5 us
  Pallas kernels  91.8 us (99%)
    pallas_call x1, Pallas kernels, on_device(): pl.pallas_call(kernel, out_shape=shapes, in_specs=[vmem] * 9 + [hbm] * 12...  90 us

profile of v2, /device:TPU:1, one launch (start us, length us, event | category | flops | bytes accessed | tf_op | source)
XLA Modules:
  0.0 92.5 jit_solution(16347994959576879201)
XLA Ops:
  0.6 90.0 %decode_layer.1 = (bf16[64,512]{1,0:T(8,128)(2,1)}, f32[64,512]{1,0:T(8,128)}, bf16[3,64,512]{2,1,0:T(8,128)(2,1)}) custom-call(bf16[16,128]{1,0:T(8,128)(2,1)} %bitcast.13, bf16[4,512]{1,0:T(4,128)(2,1)} %conv_taps.1, bf16[8,64,64]{2,1,0:T(8,128)(2,1)} %input_gate.1, bf16[8,64,64]{2,1,0:T(8,128)(2,1)} %decay_gate.1, f32[1,512]{1,0:T(1,128)} %bitcast.15, ...), custom_call_target="tpu_custom_call" | custom-call | tf_op jit(solution)/shard_map/decode_layer/pallas_call | solution.py:606
  90.7 1.8 %publish.1 = (bf16[64,512]{1,0:T(8,128)(2,1)}, f32[64,512]{1,0:T(8,128)}, bf16[3,64,512]{2,1,0:T(8,128)(2,1)}) custom-call(bf16[64,512]{1,0:T(8,128)(2,1)} %get-tuple-element.9.a, f32[64,512]{1,0:T(8,128)} %get-tuple-element.10.b, bf16[3,64,512]{2,1,0:T(8,128)(2,1)} %get-tuple-element.11.c), custom_call_target="tpu_custom_call" | custom-call | tf_op jit(solution)/shard_map/publish/pallas_call | solution.py:622
